TPU v7x, 32 devices: a whole 2x2x4 slice. The times are simulated.
32 devices in a mesh: sp: 8 (over z, y), tp: 4 (over x, core).
Axes of the slice: x: 2, y: 2, z: 4, core: 2. Of those that a mesh axis runs over, the one named last changes fastest.
Arguments:
- arriving_hidden_sum: bfloat16 [8192, 2048], P('sp'), may hold values from -40 to 40
- content_entries_clustered: bfloat16 [8192, 4096], P('sp', 'tp'), may hold values from -6 to 6
- leaving_switch_entries: bfloat16 [8192, 4096], P('sp', 'tp'), may hold values from -6 to 6
- linked_source_target_pairs: bfloat16 [8192, 8, 2, 128], P('sp', 'tp'), may hold values from -1.78125 to 1.78125
- raw_interval_length: bfloat16 [8192, 64], P('sp', 'tp'), may hold values from -5 to 5
- spike_extra_lognoise: float32 [8192, 64], P('sp', 'tp'), may hold values from -0.6 to 0
- content_filter_kernel: bfloat16 [4, 4096], P(None, 'tp'), may hold values from -3 to 3
- coupling_filter_kernel: bfloat16 [4, 8, 2, 128], P(None, 'tp'), may hold values from -3 to 3
- interval_shift_vector: float32 [64], P('tp'), may hold values from -0.5 to 0.5
- fading_speed_exponent: float32 [64], P('tp'), may hold values from -16 to -2.9
- skip_channel_factor: float32 [64], P('tp'), may hold values from 1 to 10
- cluster_rescale_vector: float32 [4096], P('tp'), may hold values from 0.1 to 1.9
- blender_final_tensor: bfloat16 [4096, 2048], P('tp'), may hold values from -0.09375 to 0.09375
- prelayer_rescale_vector: float32 [2048], replicated, may hold values from 0.1 to 1.9
- switching_linear_tensor: bfloat16 [2048, 5632], P('sp', 'tp'), may hold values from -0.125 to 0.125
- widening_linear_tensor: bfloat16 [2048, 5632], P('sp', 'tp'), may hold values from -0.125 to 0.125
- contracting_linear_tensor: bfloat16 [5632, 2048], P('tp', 'sp'), may hold values from -0.078125 to 0.078125
Outputs:
- residual_out: bfloat16 [8192, 2048], P('sp', 'tp')
All inputs are finite; a program needn't handle non-finite values.
Results may differ from a plain program's by a relative error of at most 0.012.
Values may be sent and summed in bfloat16 or wider, within the bound.
A program may use at most 128 MiB of HBM per device.

v0:
```python
import jax
import jax.numpy as jnp
from jax import lax
from jax.sharding import PartitionSpec as P

D = 2048
BLOCK_POSITIONS = 128
EPS = 1e-06
highest = lax.Precision.HIGHEST


def from_behind(block, axis, distance):
    devices = range(lax.axis_size(axis))
    route = [(i - distance, i) for i in devices if i - distance in devices]
    return lax.ppermute(block, axis, route)


def prefix(array, axis, combine, identity):
    count, place = (lax.axis_size(axis), lax.axis_index(axis))
    everything = jax.tree.map(
        lambda part, kind: lax.all_gather(part.astype(kind), axis),
        array,
        (jnp.bfloat16, jnp.bfloat16),
    )
    start = jax.tree.map(
        lambda part, zero: jnp.broadcast_to(jnp.asarray(zero, part.dtype), part.shape),
        array,
        identity,
    )

    def lap(k, before):
        reached = k < place
        new = combine(
            before, jax.tree.map(lambda part, own: part[k].astype(own.dtype), everything, array)
        )
        return jax.tree.map(lambda a, b: jnp.where(reached, a, b), new, before)

    return lax.fori_loop(0, count, lap, start)


def conv_block(values, rims, taps):
    taps_count = taps.shape[0]
    length = values.shape[0]
    padded = jnp.concatenate([rims, values], axis=0).astype(jnp.float32)
    running = jnp.zeros(values.shape, jnp.float32)
    for tap_index in range(taps_count):
        running = running + padded[tap_index : tap_index + length] * taps[tap_index].astype(
            jnp.float32
        )
    return jax.nn.silu(running).astype(jnp.bfloat16)


def combine_states(former, latter):
    return (former[0] * jnp.exp(latter[1])[:, :, None, None] + latter[0], former[1] + latter[1])


def shards(
    arriving_hidden_sum,
    content_entries_clustered,
    leaving_switch_entries,
    linked_source_target_pairs,
    raw_interval_length,
    spike_extra_lognoise,
    content_filter_kernel,
    coupling_filter_kernel,
    interval_shift_vector,
    fading_speed_exponent,
    skip_channel_factor,
    cluster_rescale_vector,
    blender_final_tensor,
    prelayer_rescale_vector,
    switching_linear_tensor,
    widening_linear_tensor,
    contracting_linear_tensor,
):
    length = content_entries_clustered.shape[0]
    heads_per_device = raw_interval_length.shape[1]
    groups_dev = linked_source_target_pairs.shape[1]
    per_group = heads_per_device // groups_dev
    head_size = content_entries_clustered.shape[1] // heads_per_device
    state_size = linked_source_target_pairs.shape[3]
    taps_count = content_filter_kernel.shape[0]
    block_count = length // BLOCK_POSITIONS
    couple_flat = linked_source_target_pairs.reshape(length, -1)
    value_rims, couple_rims = from_behind(
        (
            content_entries_clustered[length - taps_count + 1 :],
            couple_flat[length - taps_count + 1 :],
        ),
        "sp",
        1,
    )
    values = conv_block(content_entries_clustered, value_rims, content_filter_kernel)
    coupled = conv_block(
        couple_flat, couple_rims, coupling_filter_kernel.reshape(taps_count, -1)
    ).reshape(length, groups_dev, 2, state_size)
    value_blocks = values.reshape(block_count, BLOCK_POSITIONS, heads_per_device, head_size)
    write_maps = coupled[:, :, 0].reshape(block_count, BLOCK_POSITIONS, groups_dev, state_size)
    read_maps = coupled[:, :, 1].reshape(block_count, BLOCK_POSITIONS, groups_dev, state_size)
    interval_lengths = jax.nn.softplus(
        raw_interval_length.astype(jnp.float32) + interval_shift_vector
    )
    fading_log_factor = (
        -jnp.exp(fading_speed_exponent) * interval_lengths + spike_extra_lognoise
    ).reshape(block_count, BLOCK_POSITIONS, heads_per_device)
    interval_lengths = interval_lengths.reshape(block_count, BLOCK_POSITIONS, heads_per_device)
    cum_log = jnp.cumsum(fading_log_factor, axis=1)
    head_cum = jnp.swapaxes(cum_log, 1, 2)
    log_gap = head_cum[:, :, :, None] - head_cum[:, :, None, :]
    causal = jnp.tril(jnp.ones((BLOCK_POSITIONS, BLOCK_POSITIONS), bool))
    intersection = jnp.einsum(
        "blgn,bsgn->bgls", read_maps, write_maps, preferred_element_type=jnp.float32
    )
    intersection = jnp.repeat(intersection, per_group, axis=1)
    weights = (
        intersection
        * jnp.exp(jnp.where(causal, log_gap, -jnp.inf))
        * jnp.swapaxes(interval_lengths, 1, 2)[:, :, None, :]
    ).astype(jnp.bfloat16)
    within = jnp.einsum(
        "bhls,bshp->blhp", weights, value_blocks, preferred_element_type=jnp.float32
    )
    end_log = cum_log[:, -1]
    scaled = (
        value_blocks * (interval_lengths * jnp.exp(end_log[:, None, :] - cum_log))[..., None]
    ).astype(jnp.bfloat16)
    block_states = jnp.einsum(
        "blgn,blgrp->bgrpn",
        write_maps,
        scaled.reshape(block_count, BLOCK_POSITIONS, groups_dev, per_group, head_size),
        preferred_element_type=jnp.float32,
    )
    end_grouped = end_log.reshape(block_count, groups_dev, per_group)

    def carry_step(carry_state, inputs):
        block_added, block_end = inputs
        return (carry_state * jnp.exp(block_end)[:, :, None, None] + block_added, carry_state)

    zeros_state = jnp.zeros((groups_dev, per_group, head_size, state_size), jnp.float32)
    final_state, entering = lax.scan(carry_step, zeros_state, (block_states, end_grouped))
    read_wide = read_maps.astype(jnp.float32)
    carried = (
        jnp.einsum("blgn,bgrpn->blgrp", read_wide, entering, precision=highest).reshape(
            block_count, BLOCK_POSITIONS, heads_per_device, head_size
        )
        * jnp.exp(cum_log)[..., None]
    )
    device_log = jnp.sum(end_log, axis=0).reshape(groups_dev, per_group)
    incoming, _ = prefix(
        (final_state, device_log), "sp", combine_states, (zeros_state, jnp.zeros_like(device_log))
    )
    prior_log = jnp.cumsum(end_log, axis=0) - end_log
    reach_decay = jnp.exp(cum_log + prior_log[:, None, :])
    arrived = (
        jnp.einsum("blgn,grpn->blgrp", read_wide, incoming, precision=highest).reshape(
            block_count, BLOCK_POSITIONS, heads_per_device, head_size
        )
        * reach_decay[..., None]
    )
    mixer = (within + carried + arrived).reshape(
        length, heads_per_device, head_size
    ) + values.reshape(length, heads_per_device, head_size).astype(
        jnp.float32
    ) * skip_channel_factor[
        None, :, None
    ]
    gated = mixer.reshape(length, heads_per_device * head_size) * jax.nn.silu(
        leaving_switch_entries.astype(jnp.float32)
    )
    grouped = gated.reshape(length, groups_dev, per_group * head_size)
    grouped = grouped * lax.rsqrt(jnp.mean(grouped * grouped, axis=-1, keepdims=True) + EPS)
    mixed_rows = (
        grouped.reshape(length, heads_per_device * head_size) * cluster_rescale_vector
    ).astype(jnp.bfloat16)
    partial_sum = jnp.dot(mixed_rows, blender_final_tensor, preferred_element_type=jnp.float32)
    rounded = lax.optimization_barrier(partial_sum.astype(jnp.bfloat16)).astype(jnp.float32)
    col_count = D // lax.axis_size("tp")
    offset = lax.axis_index("tp") * col_count
    mixer_cols = lax.psum_scatter(
        rounded.astype(jnp.bfloat16), "tp", scatter_dimension=1, tiled=True
    ).astype(jnp.float32)
    resid_cols = lax.dynamic_slice_in_dim(arriving_hidden_sum, offset, col_count, 1)
    residual_mid = (resid_cols.astype(jnp.float32) + mixer_cols).astype(jnp.bfloat16)
    squares = residual_mid.astype(jnp.float32)
    square_sums = lax.psum(jnp.sum(squares * squares, axis=1), "tp")
    gain_cols = lax.dynamic_slice_in_dim(prelayer_rescale_vector, offset, col_count, 0)
    normed_cols = (squares * lax.rsqrt(square_sums / D + EPS)[:, None] * gain_cols).astype(
        jnp.bfloat16
    )
    normed = lax.all_gather(normed_cols, "tp", axis=1, tiled=True)
    gate_pre = jnp.dot(
        normed,
        lax.all_gather(switching_linear_tensor, "sp", axis=0, tiled=True),
        preferred_element_type=jnp.float32,
    )
    up_pre = jnp.dot(
        normed,
        lax.all_gather(widening_linear_tensor, "sp", axis=0, tiled=True),
        preferred_element_type=jnp.float32,
    )
    hidden = (jax.nn.silu(gate_pre) * up_pre).astype(jnp.bfloat16)
    down_terms = jnp.dot(
        hidden,
        lax.all_gather(contracting_linear_tensor, "sp", axis=1, tiled=True),
        preferred_element_type=jnp.float32,
    )
    down_rounded = lax.optimization_barrier(down_terms.astype(jnp.bfloat16)).astype(jnp.float32)
    mlp_cols = lax.psum_scatter(
        down_rounded.astype(jnp.bfloat16), "tp", scatter_dimension=1, tiled=True
    ).astype(jnp.float32)
    return (residual_mid.astype(jnp.float32) + 0.5 * mlp_cols).astype(jnp.bfloat16)


def solution(mesh):
    placed = (
        P("sp", None),
        P("sp", "tp"),
        P("sp", "tp"),
        P("sp", "tp", None, None),
        P("sp", "tp"),
        P("sp", "tp"),
        P(None, "tp"),
        P(None, "tp", None, None),
        P("tp"),
        P("tp"),
        P("tp"),
        P("tp"),
        P("tp", None),
        P(),
        P("sp", "tp"),
        P("sp", "tp"),
        P("tp", "sp"),
    )
    return jax.shard_map(
        shards, mesh=mesh, in_specs=placed, out_specs=P("sp", "tp"), check_vma=False
    )
```

profile of v0, /device:TPU:0, one launch (start us, length us, event | category | flops | bytes accessed | tf_op | source)
XLA Modules:
  0.0 612.9 jit_solution(5842465863375640701)
XLA Ops:
  8.2 4.9 collective-permute-start
  14.6 4.1 collective-permute-start.1
  20.6 23.3 %fusion.43 = f32[8,128,16]{2,0,1:T(8,128)S(1)} fusion(f32[8,128,16]{2,0,1:T(8,128)S(1)} %copy.81), kind=kOutput, calls=%fused_computation.88 | output fusion | flops 2080768 | bytes 131072 | tf_op jit(solution)/shard_map/jit(cumsum)/reduce_window_sum | solution.py:107
  44.3 1.5 slice_convert_fusion.3
  45.8 1.3 fusion.42
  47.2 2.9 copy.74
  50.0 3.7 copy.76
  53.7 1.2 convert.10
  54.9 1.2 convert.11
  56.1 1.3 convert.12
  57.4 1.2 convert.13
  58.6 1.8 maximum_convert_fusion.1
  60.4 3.0 multiply_convert_fusion.5
  64.5 2.0 copy.78
  66.6 1.2 maximum_convert_fusion
  67.9 4.5 convert_bitcast_fusion
  74.4 2.7 fusion.25
  77.1 16.2 %while.27 = (s32[]{:T(128)}, f32[2,8,64,128]{3,2,1,0:T(8,128)S(1)}, f32[8,2,8,64,128]{4,3,2,1,0:T(8,128)}, f32[8,2,8]{2,1,0:T(2,128)S(1)}, f32[8,2,8,64,128]{4,3,2,1,0:T(8,128)}, /*index=5*/s32[]{:T(128)}, s32[]{:T(128)}) while((s32[]{:T(128)}, f32[2,8,64,128]{3,2,1,0:T(8,128)S(1)}, f32[8,2,8,64,128]{4,3,2,1,0:T(8,128)}, ...), condition=%wide.region_2.3_spmd.clone, body=%wide.region_1.2_spmd.clone.sunk | while | flops 524291 | bytes 2622240 | solution.py:140
  77.9 1.2 bitcast_add_fusion.3
  82.0 1.2 bitcast_add_fusion.3
  95.4 1.2 copy.92
  96.6 1.2 copy.94
  98.1 4.0 copy.96
  102.2 17.5 %all_gather.22 = bf16[8,2,8]{2,1,0:T(2,128)(2,1)S(1)} all-gather(bf16[1,2,8]{2,1,0:T(2,128)(2,1)S(1)} %convert_element_type.180), channel_id=1, replica_groups=mesh['sp'=8,'tp'=4] {'sp'}, dimensions={0}, use_global_device_ids=true | all-gather | bytes 288 | tf_op jit(solution)/shard_map/all_gather | solution.py:21
  119.7 1.3 copy.77
  121.0 2.6 fusion.34
  123.6 2.0 copy.106
  125.7 3.5 fusion.31
  129.1 13.8 %all-gather.15.cloned.1.call-done = bf16[16,8,64,128]{3,2,1,0:T(8,128)(2,1)} async-done(((bf16[2,8,64,128]{3,2,1,0:T(8,128)(2,1)}), bf16[16,8,64,128]{3,2,1,0:T(8,128)(2,1)}) %all-gather.15.cloned.1.call-update) | async-done | bytes 2097168 | tf_op jit(solution)/shard_map/all_gather | solution.py:21
  143.0 9.0 %while.28 = (s32[]{:T(128)}, f32[2,8,64,128]{3,2,1,0:T(8,128)S(1)}, s32[]{:T(128)}, bf16[8,2,8]{2,1,0:T(2,128)(2,1)S(1)}, bf16[8,2,8,64,128]{4,3,2,1,0:T(8,128)(2,1)}, /*index=5*/s32[]{:T(128)}, s32[]{:T(128)}) while((s32[]{:T(128)}, f32[2,8,64,128]{3,2,1,0:T(8,128)S(1)}, s32[]{:T(128)}, bf16[8,2,8]{2,1,0:T(2,128)(2,1)S(1)}, ...), condition=%wide.region_5.6_spmd.clone, body=%wide.region_4.5_spmd.clone.sunk | while | flops 655380 | bytes 1310985 | solution.py:38
  152.0 1.8 convolution_bitcast_fusion
  157.9 6.0 fusion.12
  164.0 5.6 copy.95
  169.6 2.8 bitcast_reduce_fusion
  172.9 1.7 copy-done.11
  174.6 6.2 %convolution_convert_fusion.1 = bf16[1024,2048]{1,0:T(8,128)(2,1)} fusion(bf16[1024,1024]{0,1:T(8,128)(2,1)S(1)} %fusion.11, bf16[1024,2048]{1,0:T(8,128)(2,1)S(1)} %copy-done.11), kind=kOutput, calls=%fused_computation.39 | convolution fusion | flops 4297064448 | bytes 10485760 | tf_op jit(solution)/shard_map/dot_general | solution.py:175
  182.6 41.3 %reduce-scatter.3.cloned.1.call-done = bf16[1024,512]{1,0:T(8,128)(2,1)} async-done(((bf16[1024,2048]{1,0:T(8,128)(2,1)}), bf16[1024,512]{1,0:T(8,128)(2,1)}) %reduce-scatter.3.cloned.1.call-update) | async-done | bytes 1048592 | tf_op jit(solution)/shard_map/reduce_scatter | solution.py:179
  224.0 2.0 fusion.18
  226.0 5.8 psum.7
  231.7 1.3 fusion.20
  234.2 84.3 %all-gather.9.cloned.1.call-done = bf16[2048,1408]{1,0:T(8,128)(2,1)} async-done(((bf16[256,1408]{1,0:T(8,128)(2,1)}), bf16[2048,1408]{1,0:T(8,128)(2,1)}) %all-gather.9.cloned.1.call-update) | async-done | bytes 5767184 | tf_op jit(solution)/shard_map/all_gather | solution.py:193
  318.5 34.1 %all-gather.7.cloned.1.call-done = bf16[1024,2048]{1,0:T(8,128)(2,1)} async-done(((bf16[1024,512]{1,0:T(8,128)(2,1)}), bf16[1024,2048]{1,0:T(8,128)(2,1)}) %all-gather.7.cloned.1.call-update) | async-done | bytes 4194320 | tf_op jit(solution)/shard_map/all_gather | solution.py:190
  352.6 11.7 %fusion.44 = f32[1024,1408]{1,0:T(8,128)} fusion(bf16[1024,2048]{1,0:T(8,128)(2,1)} %all-gather.7.cloned.1.call-done, bf16[2048,1408]{1,0:T(8,128)(2,1)} %all-gather.9.cloned.1.call-done), kind=kOutput, calls=%fused_computation.89 | convolution fusion | flops 5905580032 | bytes 15728640 | tf_op jit(solution)/shard_map/dot_general | solution.py:191
  364.3 82.7 %all-gather.11.cloned.1.call-done = bf16[2048,1408]{1,0:T(8,128)(2,1)} async-done(((bf16[256,1408]{1,0:T(8,128)(2,1)}), bf16[2048,1408]{1,0:T(8,128)(2,1)}) %all-gather.11.cloned.1.call-update) | async-done | bytes 5767184 | tf_op jit(solution)/shard_map/all_gather | solution.py:198
  447.0 93.2 %all-gather.13.cloned.1.call-done = bf16[1408,2048]{1,0:T(8,128)(2,1)} async-done(((bf16[1408,256]{1,0:T(8,128)(2,1)}), bf16[1408,2048]{1,0:T(8,128)(2,1)}) %all-gather.13.cloned.1.call-update) | async-done | bytes 5767184 | tf_op jit(solution)/shard_map/all_gather | solution.py:204
  540.2 20.5 %convolution_convert_fusion = bf16[1024,2048]{1,0:T(8,128)(2,1)} fusion(bf16[1408,2048]{1,0:T(8,128)(2,1)} %all-gather.13.cloned.1.call-done, f32[1024,1408]{1,0:T(8,128)} %fusion.44, bf16[1024,2048]{1,0:T(8,128)(2,1)} %all-gather.7.cloned.1.call-done, bf16[2048,1408]{1,0:T(8,128)(2,1)} %all-gather.11.cloned.1.call-done), kind=kOutput, calls=%fused_computation.38 | convolution fusion | flops 11821907968 | bytes 25690112 | tf_op jit(solution)/shard_map/dot_general | solution.py:202
  560.8 42.7 %reduce-scatter.5.cloned.1.call-done = bf16[1024,512]{1,0:T(8,128)(2,1)} async-done(((bf16[1024,2048]{1,0:T(8,128)(2,1)}), bf16[1024,512]{1,0:T(8,128)(2,1)}) %reduce-scatter.5.cloned.1.call-update) | async-done | bytes 1048592 | tf_op jit(solution)/shard_map/reduce_scatter | solution.py:208
  603.5 2.5 fusion.21
  (113 shorter events, 41.1 us)
Async XLA Ops:
  6.5 136.4 %all-gather.15.cloned.1.call-start = ((), (), s32[]{:S(2)}) async-start(), calls=%async_computation.8 | async-start | bytes 2359296 | tf_op jit(solution)/shard_map/all_gather | solution.py:21
  8.2 58.4 %collective-permute-start = (bf16[3,1024]{0,1:T(8,128)(2,1)}, bf16[3,1024]{0,1:T(8,128)(2,1)S(1)}, u32[]{:S(2)}, u32[]{:S(2)}) collective-permute-start(bf16[3,1024]{0,1:T(8,128)(2,1)} %copy.73), channel_id=1, source_target_pairs={{0,4},{4,8},{8,12},{12,16},{16,20},{20,24},{24,28},{1,5},{5,9},{9,... | collective-permute-start | bytes 18440 | tf_op jit(solution)/shard_map/ppermute | solution.py:15
  14.6 44.0 %collective-permute-start.1 = (bf16[3,512]{0,1:T(8,128)(2,1)}, bf16[3,512]{0,1:T(8,128)(2,1)}, u32[]{:S(2)}, u32[]{:S(2)}) collective-permute-start(bf16[3,512]{0,1:T(8,128)(2,1)} %bitcast.4), channel_id=1, source_target_pairs={{0,4},{4,8},{8,12},{12,16},{16,20},{20,24},{24,28},{1,5},{5,9},{9,... | collective-permute-start | bytes 9224 | tf_op jit(solution)/shard_map/ppermute | solution.py:15
  66.6 1.2 copy-start.6
  66.6 1.2 copy-start.7
  66.6 1.3 copy-start.8
  73.3 1.0 copy-start.3
  94.1 8.0 %copy-start.10 = (f32[16]{0:T(128)S(1)}, f32[16]{0:T(128)}, u32[]{:S(2)}) copy-start(f32[16]{0:T(128)} %param.31) | copy-start | bytes 196
  94.1 129.9 %reduce-scatter.3.cloned.1.call-start = ((), (), s32[]{:S(2)}) async-start(), calls=%async_computation.2 | async-start | bytes 5242880 | tf_op jit(solution)/shard_map/reduce_scatter | solution.py:179
  121.0 4.7 copy-start.5
  153.8 1.2 copy-start.4
  155.1 2.2 copy-start
  155.1 2.9 copy-start.2
  164.0 5.6 copy-start.1
  169.6 2.9 copy-start.9
  172.4 2.2 copy-start.11
  180.9 137.6 %all-gather.9.cloned.1.call-start = ((), (), s32[]{:S(2)}) async-start(), calls=%async_computation.4 | async-start | bytes 6488064 | tf_op jit(solution)/shard_map/all_gather | solution.py:193
  181.6 171.0 %all-gather.7.cloned.1.call-start = ((), (), s32[]{:S(2)}) async-start(), calls=%async_computation.3 | async-start | bytes 5242880 | tf_op jit(solution)/shard_map/all_gather | solution.py:190
  233.0 213.9 %all-gather.11.cloned.1.call-start = ((), (), s32[]{:S(2)}) async-start(), calls=%async_computation.5 | async-start | bytes 6488064 | tf_op jit(solution)/shard_map/all_gather | solution.py:198
  233.6 306.6 %all-gather.13.cloned.1.call-start = ((), (), s32[]{:S(2)}) async-start(), calls=%async_computation.6 | async-start | bytes 6488064 | tf_op jit(solution)/shard_map/all_gather | solution.py:204
  234.2 369.3 %reduce-scatter.5.cloned.1.call-start = ((), (), s32[]{:S(2)}) async-start(), calls=%async_computation.7 | async-start | bytes 5242880 | tf_op jit(solution)/shard_map/reduce_scatter | solution.py:208
Sparse Core Ops, SparseCore 0:
  94.2 48.7 all-gather.14
  181.0 42.9 reduce-scatter.2
  226.2 92.2 all-gather.8
  319.9 32.6 all-gather.6
  354.6 92.3 all-gather.10
  448.9 91.2 all-gather.12
  560.9 42.5 reduce-scatter.4
where the time goes:
time: 615 us; the launch traced here: 613 us
  waiting for transfers between devices  394 us (64%)
  other arithmetic  78.2 us (13%)
  matrix products  55.1 us (9%)
  local copies, waits for them, and re-layouts  38.7 us (6%)
  blocking collectives  23.2 us (4%)
  between operations  13.8 us (2%)
  starting transfers between devices  9.44 us (2%)
    all_gather x1, waiting for transfers between devices, shards(): lax.all_gather(contracting_linear_tensor, 'sp', axis=1, tiled=True)  93.2 us
    all_gather x1, waiting for transfers between devices, shards(): lax.all_gather(switching_linear_tensor, 'sp', axis=0, tiled=True)  84.3 us
    all_gather x1, waiting for transfers between devices, shards(): lax.all_gather(widening_linear_tensor, 'sp', axis=0, tiled=True)  82.7 us
    reduce_scatter x1, waiting for transfers between devices, shards(): lax.psum_scatter(down_rounded.astype(jnp.bfloat16), 'tp', scatter_dimensi...  42.7 us
    reduce_scatter x1, waiting for transfers between devices, shards(): lax.psum_scatter(rounded.astype(jnp.bfloat16), 'tp', scatter_dimension=1,...  41.3 us
    all_gather x1, waiting for transfers between devices, shards(): normed = lax.all_gather(normed_cols, 'tp', axis=1, tiled=True)  34.1 us
    another operation x1, other arithmetic, shards(): cum_log = jnp.cumsum(fading_log_factor, axis=1)  23.3 us
    dot_general x1, matrix products, shards(): jnp.dot(hidden, lax.all_gather(contracting_linear_tensor, 'sp', axis=1, t...  20.5 us
  transfers between devices with their start and end apart: 9, of which 7 were waited for; matrix products, arithmetic and copies ran while one was open for 13% of the time, Pallas kernels for 0%

commit v1 on v0

--- a/solution.py
+++ b/solution.py
@@ -7,6 +7,24 @@
 BLOCK_POSITIONS = 128
 EPS = 1e-06
 highest = lax.Precision.HIGHEST
+
+
+def _advance_ticks(sheet):
+    degree = jax.lax.axis_size("tp")
+    lanes = list(map(lambda j0: (j0, (j0 + 1) % degree), range(degree)))
+
+    def balance_shelves_by_axis(reply):
+        if len(reply) == degree:
+            return reply
+        return balance_shelves_by_axis(
+            [jax.lax.ppermute(reply[0], axis_name="tp", perm=lanes), *reply]
+        )
+
+    return jnp.roll(
+        jnp.concatenate(balance_shelves_by_axis([sheet]), 1),
+        (jax.lax.axis_index("tp") + 1) * sheet.shape[1],
+        1,
+    )
 
 
 def from_behind(block, axis, distance):
@@ -187,7 +205,7 @@
     normed_cols = (squares * lax.rsqrt(square_sums / D + EPS)[:, None] * gain_cols).astype(
         jnp.bfloat16
     )
-    normed = lax.all_gather(normed_cols, "tp", axis=1, tiled=True)
+    normed = _advance_ticks(normed_cols)
     gate_pre = jnp.dot(
         normed,
         lax.all_gather(switching_linear_tensor, "sp", axis=0, tiled=True),

time: 615 us -> 579 us (0.941)
  waiting for transfers between devices: 394 us -> 347 us
  local copies, waits for them, and re-layouts: 38.7 us -> 48 us
    all_gather x1, waiting for transfers between devices: 84.3 us -> 31.7 us  [shards(): lax.all_gather(switching_linear_tensor, 'sp', axis=0, tiled=True)]
    ppermute x0 -> x3, waiting for transfers between devices: none -> 42.8 us  [balance_shelves_by_axis(): jax.lax.ppermute(reply[0], axis_name='tp', perm=lanes)]
    all_gather x1 -> x0, waiting for transfers between devices: 34.1 us -> none  [shards(): normed = lax.all_gather(normed_cols, 'tp', axis=1, tiled=True)]
    all_gather x1, waiting for transfers between devices: 93.2 us -> 81.5 us  [shards(): lax.all_gather(contracting_linear_tensor, 'sp', axis=1, tiled=True)]
    all_gather x1, waiting for transfers between devices: 82.7 us -> 92.6 us  [shards(): lax.all_gather(widening_linear_tensor, 'sp', axis=0, tiled=True)]
    unnamed x31 -> x37, local copies, waits for them, and re-layouts: 18.3 us -> 27.5 us
  transfers between devices with their start and end apart: 9 -> 11, of which waited for: 7 -> 9; matrix products, arithmetic and copies ran while one was open for 13% -> 16% of each run, Pallas kernels for 0% -> 0%
where the time goes in v1:
time: 579 us; the launch traced here: 577 us
  waiting for transfers between devices  347 us (60%)
  other arithmetic  79.9 us (14%)
  matrix products  55.2 us (10%)
  local copies, waits for them, and re-layouts  48 us (8%)
  blocking collectives  23.2 us (4%)
  between operations  13.8 us (2%)
  starting transfers between devices  9.46 us (2%)
    all_gather x1, waiting for transfers between devices, shards(): lax.all_gather(widening_linear_tensor, 'sp', axis=0, tiled=True)  92.6 us
    all_gather x1, waiting for transfers between devices, shards(): lax.all_gather(contracting_linear_tensor, 'sp', axis=1, tiled=True)  81.5 us
    ppermute x3, waiting for transfers between devices, balance_shelves_by_axis(): jax.lax.ppermute(reply[0], axis_name='tp', perm=lanes)  42.8 us
    reduce_scatter x1, waiting for transfers between devices, shards(): lax.psum_scatter(down_rounded.astype(jnp.bfloat16), 'tp', scatter_dimensi...  42.7 us
    reduce_scatter x1, waiting for transfers between devices, shards(): lax.psum_scatter(rounded.astype(jnp.bfloat16), 'tp', scatter_dimension=1,...  40.4 us
    all_gather x1, waiting for transfers between devices, shards(): lax.all_gather(switching_linear_tensor, 'sp', axis=0, tiled=True)  31.7 us
    unnamed x37, local copies, waits for them, and re-layouts  27.5 us
    another operation x1, other arithmetic, shards(): cum_log = jnp.cumsum(fading_log_factor, axis=1)  23.3 us
  transfers between devices with their start and end apart: 11, of which 9 were waited for; matrix products, arithmetic and copies ran while one was open for 16% of the time, Pallas kernels for 0%

profile of v1, /device:TPU:0, one launch (start us, length us, event | category | flops | bytes accessed | tf_op | source)
XLA Modules:
  0.0 577.0 jit_solution(13001684687960305276)
XLA Ops:
  8.2 4.9 collective-permute-start
  14.6 4.1 collective-permute-start.1
  20.6 23.3 %fusion.51 = f32[8,128,16]{2,0,1:T(8,128)S(1)} fusion(f32[8,128,16]{2,0,1:T(8,128)S(1)} %copy.81), kind=kOutput, calls=%fused_computation.102 | output fusion | flops 2080768 | bytes 131072 | tf_op jit(solution)/shard_map/jit(cumsum)/reduce_window_sum | solution.py:125
  44.3 1.5 slice_convert_fusion.3
  45.8 1.3 fusion.50
  47.2 2.9 copy.74
  50.0 3.7 copy.76
  53.7 1.2 convert.10
  54.9 1.2 convert.11
  56.1 1.3 convert.12
  57.4 1.2 convert.13
  58.6 1.8 maximum_convert_fusion.1
  60.4 3.0 multiply_convert_fusion.5
  64.5 2.0 copy.78
  67.9 4.5 convert_bitcast_fusion
  74.4 2.7 fusion.31
  77.1 16.2 %while.27 = (s32[]{:T(128)}, f32[2,8,64,128]{3,2,1,0:T(8,128)S(1)}, f32[8,2,8,64,128]{4,3,2,1,0:T(8,128)}, f32[8,2,8]{2,1,0:T(2,128)S(1)}, f32[8,2,8,64,128]{4,3,2,1,0:T(8,128)}, /*index=5*/s32[]{:T(128)}, s32[]{:T(128)}) while((s32[]{:T(128)}, f32[2,8,64,128]{3,2,1,0:T(8,128)S(1)}, f32[8,2,8,64,128]{4,3,2,1,0:T(8,128)}, ...), condition=%wide.region_2.3_spmd.clone, body=%wide.region_1.2_spmd.clone.sunk | while | flops 524291 | bytes 2622240 | solution.py:158
  98.1 4.0 copy.96
  102.2 17.5 %all_gather.19 = bf16[8,2,8]{2,1,0:T(2,128)(2,1)S(1)} all-gather(bf16[1,2,8]{2,1,0:T(2,128)(2,1)S(1)} %convert_element_type.180), channel_id=1, replica_groups=mesh['sp'=8,'tp'=4] {'sp'}, dimensions={0}, use_global_device_ids=true | all-gather | bytes 288 | tf_op jit(solution)/shard_map/all_gather | solution.py:39
  119.7 1.3 copy.77
  121.0 2.6 fusion.40
  123.6 2.0 copy.106
  125.7 3.5 fusion.37
  129.1 13.8 %all-gather.12.cloned.1.call-done = bf16[16,8,64,128]{3,2,1,0:T(8,128)(2,1)} async-done(((bf16[2,8,64,128]{3,2,1,0:T(8,128)(2,1)}), bf16[16,8,64,128]{3,2,1,0:T(8,128)(2,1)}) %all-gather.12.cloned.1.call-update) | async-done | bytes 2097168 | tf_op jit(solution)/shard_map/all_gather | solution.py:39
  143.0 9.0 %while.28 = (s32[]{:T(128)}, f32[2,8,64,128]{3,2,1,0:T(8,128)S(1)}, s32[]{:T(128)}, bf16[8,2,8]{2,1,0:T(2,128)(2,1)S(1)}, bf16[8,2,8,64,128]{4,3,2,1,0:T(8,128)(2,1)}, /*index=5*/s32[]{:T(128)}, s32[]{:T(128)}) while((s32[]{:T(128)}, f32[2,8,64,128]{3,2,1,0:T(8,128)S(1)}, s32[]{:T(128)}, bf16[8,2,8]{2,1,0:T(2,128)(2,1)S(1)}, ...), condition=%wide.region_5.6_spmd.clone, body=%wide.region_4.5_spmd.clone.sunk | while | flops 655380 | bytes 1310985 | solution.py:56
  152.0 1.8 convolution_bitcast_fusion
  157.9 6.0 %fusion.12 = f32[8,128,16,64]{1,3,2,0:T(8,128)} fusion(f32[8,128,16,64]{1,3,2,0:T(8,128)S(1)} %bitcast.129, f32[8,128,16,64]{1,3,2,0:T(8,128)S(1)} %bitcast.128, f32[8,128,16]{1,2,0:T(8,128)S(1)} %copy.94, f32[8,128,16]{1,2,0:T(8,128)S(1)} %copy.92, f32[8,16,128,128]{3,2,1,0:T(8,128)S(1)} %bitcast.126, f32[8,16,128]{2,1,0:T(8,128)S(1)} %copy.84, ...), kind=kOutput, calls=%fused_computation.30 | convolution fusion | flops 283115520 | bytes 23347200 | tf_op jit(solution)/shard_map/bhls,bshp->blhp/dot_general | solution.py:138
  164.0 5.6 copy.95
  169.6 2.8 bitcast_reduce_fusion
  172.9 1.7 copy-done.11
  174.6 6.2 %convolution_convert_fusion.1 = bf16[1024,2048]{1,0:T(8,128)(2,1)} fusion(bf16[1024,1024]{0,1:T(8,128)(2,1)S(1)} %fusion.11, bf16[1024,2048]{1,0:T(8,128)(2,1)S(1)} %copy-done.11), kind=kOutput, calls=%fused_computation.39 | convolution fusion | flops 4297064448 | bytes 10485760 | tf_op jit(solution)/shard_map/dot_general | solution.py:193
  183.5 40.4 %reduce-scatter.3.cloned.1.call-done = bf16[1024,512]{1,0:T(8,128)(2,1)} async-done(((bf16[1024,2048]{1,0:T(8,128)(2,1)}), bf16[1024,512]{1,0:T(8,128)(2,1)}) %reduce-scatter.3.cloned.1.call-update) | async-done | bytes 1048592 | tf_op jit(solution)/shard_map/reduce_scatter | solution.py:197
  223.9 2.0 fusion.24
  225.9 5.8 psum.7
  232.1 14.2 %collective-permute-done.2 = bf16[1024,512]{1,0:T(8,128)(2,1)S(1)} collective-permute-done((bf16[1024,512]{1,0:T(8,128)(2,1)S(1)}, bf16[1024,512]{1,0:T(8,128)(2,1)S(1)}, u32[]{:S(2)}, u32[]{:S(2)}) %collective-permute-start.2) | collective-permute-done | bytes 1048608 | tf_op jit(solution)/shard_map/ppermute | solution.py:20
  246.3 14.2 %collective-permute-done.3 = bf16[1024,512]{1,0:T(8,128)(2,1)S(1)} collective-permute-done((bf16[1024,512]{1,0:T(8,128)(2,1)S(1)}, bf16[1024,512]{1,0:T(8,128)(2,1)S(1)}, u32[]{:S(2)}, u32[]{:S(2)}) %collective-permute-start.3) | collective-permute-done | bytes 1048608 | tf_op jit(solution)/shard_map/ppermute | solution.py:20
  260.5 14.3 %collective-permute-done.4 = bf16[1024,512]{1,0:T(8,128)(2,1)} collective-permute-done((bf16[1024,512]{1,0:T(8,128)(2,1)S(1)}, bf16[1024,512]{1,0:T(8,128)(2,1)}, u32[]{:S(2)}, u32[]{:S(2)}) %collective-permute-start.4) | collective-permute-done | bytes 1048608 | tf_op jit(solution)/shard_map/ppermute | solution.py:20
  274.8 2.3 constant_dynamic-update-slice_fusion.7
  279.4 1.4 constant_dynamic-update-slice_fusion.4
  280.8 2.3 constant_dynamic-update-slice_fusion.3
  285.5 1.3 constant_dynamic-update-slice_fusion
  286.8 31.7 %all-gather.6.cloned.1.call-done = bf16[2048,1408]{1,0:T(8,128)(2,1)} async-done(((bf16[256,1408]{1,0:T(8,128)(2,1)}), bf16[2048,1408]{1,0:T(8,128)(2,1)}) %all-gather.6.cloned.1.call-update) | async-done | bytes 5767184 | tf_op jit(solution)/shard_map/all_gather | solution.py:211
  318.5 11.7 %fusion.20 = f32[1024,1408]{1,0:T(8,128)} fusion(bf16[2048,1408]{1,0:T(8,128)(2,1)} %all-gather.6.cloned.1.call-done, bf16[1024,4096]{1,0:T(8,128)(2,1)} %constant_dynamic-update-slice_fusion, s32[]{:T(128)S(6)} %select_n.53), kind=kOutput, calls=%fused_computation.42 | convolution fusion | flops 5905580032 | bytes 15728644 | tf_op jit(solution)/shard_map/dot_general | solution.py:209
  330.2 81.5 %all-gather.10.cloned.1.call-done = bf16[1408,2048]{1,0:T(8,128)(2,1)} async-done(((bf16[1408,256]{1,0:T(8,128)(2,1)}), bf16[1408,2048]{1,0:T(8,128)(2,1)}) %all-gather.10.cloned.1.call-update) | async-done | bytes 5767184 | tf_op jit(solution)/shard_map/all_gather | solution.py:222
  411.7 92.6 %all-gather.8.cloned.1.call-done = bf16[2048,1408]{1,0:T(8,128)(2,1)} async-done(((bf16[256,1408]{1,0:T(8,128)(2,1)}), bf16[2048,1408]{1,0:T(8,128)(2,1)}) %all-gather.8.cloned.1.call-update) | async-done | bytes 5767184 | tf_op jit(solution)/shard_map/all_gather | solution.py:216
  504.3 20.6 %convolution_convert_fusion = bf16[1024,2048]{1,0:T(8,128)(2,1)} fusion(bf16[1408,2048]{1,0:T(8,128)(2,1)} %all-gather.10.cloned.1.call-done, f32[1024,1408]{1,0:T(8,128)} %fusion.20, bf16[2048,1408]{1,0:T(8,128)(2,1)} %all-gather.8.cloned.1.call-done, bf16[1024,4096]{1,0:T(8,128)(2,1)} %constant_dynamic-update-slice_fusion, s32[]{:T(128)S(6)} %select_n.53), kind=kOutput, calls=%fused_computation.38 | convolution fusion | flops 11821907968 | bytes 25690116 | tf_op jit(solution)/shard_map/dot_general | solution.py:220
  524.9 42.7 %reduce-scatter.5.cloned.1.call-done = bf16[1024,512]{1,0:T(8,128)(2,1)} async-done(((bf16[1024,2048]{1,0:T(8,128)(2,1)}), bf16[1024,512]{1,0:T(8,128)(2,1)}) %reduce-scatter.5.cloned.1.call-update) | async-done | bytes 1048592 | tf_op jit(solution)/shard_map/reduce_scatter | solution.py:226
  567.6 2.5 fusion.27
  (124 shorter events, 51.8 us)
Async XLA Ops:
  6.5 136.4 %all-gather.12.cloned.1.call-start = ((), (), s32[]{:S(2)}) async-start(), calls=%async_computation.7 | async-start | bytes 2359296 | tf_op jit(solution)/shard_map/all_gather | solution.py:39
  8.2 58.4 %collective-permute-start = (bf16[3,1024]{0,1:T(8,128)(2,1)}, bf16[3,1024]{0,1:T(8,128)(2,1)S(1)}, u32[]{:S(2)}, u32[]{:S(2)}) collective-permute-start(bf16[3,1024]{0,1:T(8,128)(2,1)} %copy.73), channel_id=1, source_target_pairs={{0,4},{4,8},{8,12},{12,16},{16,20},{20,24},{24,28},{1,5},{5,9},{9,... | collective-permute-start | bytes 18440 | tf_op jit(solution)/shard_map/ppermute | solution.py:33
  14.6 44.0 %collective-permute-start.1 = (bf16[3,512]{0,1:T(8,128)(2,1)}, bf16[3,512]{0,1:T(8,128)(2,1)}, u32[]{:S(2)}, u32[]{:S(2)}) collective-permute-start(bf16[3,512]{0,1:T(8,128)(2,1)} %bitcast.4), channel_id=1, source_target_pairs={{0,4},{4,8},{8,12},{12,16},{16,20},{20,24},{24,28},{1,5},{5,9},{9,... | collective-permute-start | bytes 9224 | tf_op jit(solution)/shard_map/ppermute | solution.py:33
  66.6 1.2 copy-start.6
  66.6 1.2 copy-start.7
  66.6 1.3 copy-start.8
  73.3 1.0 copy-start.3
  94.1 8.0 %copy-start.10 = (f32[16]{0:T(128)S(1)}, f32[16]{0:T(128)}, u32[]{:S(2)}) copy-start(f32[16]{0:T(128)} %param.31) | copy-start | bytes 196
  94.1 129.8 %reduce-scatter.3.cloned.1.call-start = ((), (), s32[]{:S(2)}) async-start(), calls=%async_computation.2 | async-start | bytes 5242880 | tf_op jit(solution)/shard_map/reduce_scatter | solution.py:197
  121.0 4.7 copy-start.5
  153.8 1.2 copy-start.4
  155.1 2.2 copy-start
  155.1 2.9 copy-start.2
  164.0 5.6 copy-start.1
  169.6 2.9 copy-start.9
  172.4 2.2 copy-start.11
  180.8 137.6 %all-gather.6.cloned.1.call-start = ((), (), s32[]{:S(2)}) async-start(), calls=%async_computation.3 | async-start | bytes 6488064 | tf_op jit(solution)/shard_map/all_gather | solution.py:211
  181.6 230.1 %all-gather.10.cloned.1.call-start = ((), (), s32[]{:S(2)}) async-start(), calls=%async_computation.5 | async-start | bytes 6488064 | tf_op jit(solution)/shard_map/all_gather | solution.py:222
  182.1 322.1 %all-gather.8.cloned.1.call-start = ((), (), s32[]{:S(2)}) async-start(), calls=%async_computation.4 | async-start | bytes 6488064 | tf_op jit(solution)/shard_map/all_gather | solution.py:216
  182.7 384.9 %reduce-scatter.5.cloned.1.call-start = ((), (), s32[]{:S(2)}) async-start(), calls=%async_computation.6 | async-start | bytes 5242880 | tf_op jit(solution)/shard_map/reduce_scatter | solution.py:226
  232.0 14.3 %collective-permute-start.2 = (bf16[1024,512]{1,0:T(8,128)(2,1)S(1)}, bf16[1024,512]{1,0:T(8,128)(2,1)S(1)}, u32[]{:S(2)}, u32[]{:S(2)}) collective-permute-start(bf16[1024,512]{1,0:T(8,128)(2,1)S(1)} %fusion.26), channel_id=1, source_target_pairs={{0,1},{1,2},{2,3},{3,0},{4,5},{5,6},{6,7},{7,4},{8,9},{9,10},{10,1... | collective-permute-start | bytes 3145736 | tf_op jit(solution)/shard_map/ppermute | solution.py:20
  246.3 14.2 %collective-permute-start.3 = (bf16[1024,512]{1,0:T(8,128)(2,1)S(1)}, bf16[1024,512]{1,0:T(8,128)(2,1)S(1)}, u32[]{:S(2)}, u32[]{:S(2)}) collective-permute-start(bf16[1024,512]{1,0:T(8,128)(2,1)S(1)} %collective-permute-done.2), channel_id=1, source_target_pairs={{0,1},{1,2},{2,3},{3,0},{4,5},{5,6},{6,7},{7,4},{8,9},{9,10},{10,1... | collective-permute-start | bytes 3145736 | tf_op jit(solution)/shard_map/ppermute | solution.py:20
  260.5 14.3 %collective-permute-start.4 = (bf16[1024,512]{1,0:T(8,128)(2,1)S(1)}, bf16[1024,512]{1,0:T(8,128)(2,1)}, u32[]{:S(2)}, u32[]{:S(2)}) collective-permute-start(bf16[1024,512]{1,0:T(8,128)(2,1)S(1)} %collective-permute-done.3), channel_id=1, source_target_pairs={{0,1},{1,2},{2,3},{3,0},{4,5},{5,6},{6,7},{7,4},{8,9},{9,10},{10,1... | collective-permute-start | bytes 3145736 | tf_op jit(solution)/shard_map/ppermute | solution.py:20
Sparse Core Ops, SparseCore 0:
  94.2 48.7 all-gather.11
  180.9 42.9 reduce-scatter.2
  226.1 92.2 all-gather.5
  320.4 91.3 all-gather.9
  413.7 90.4 all-gather.7
  525.0 42.5 reduce-scatter.4
